TPU v7x, 128 devices: a whole 4x4x4 slice. The times are simulated.
128 devices in a mesh: sp: 32 (over z, y, core), tp: 4 (over x).
Axes of the slice: x: 4, y: 4, z: 4, core: 2. Of those that a mesh axis runs over, the one named last changes fastest.
Arguments:
- inputs: bfloat16 [16384, 3072], P('sp', 'tp'), may hold values from -6 to 6
- w_query: bfloat16 [3072, 1536], P(None, 'tp'), may hold values from -0.109375 to 0.109375
- w_key: bfloat16 [3072, 1536], P(None, 'tp'), may hold values from -0.109375 to 0.109375
- w_value: bfloat16 [3072, 1536], P(None, 'tp'), may hold values from -0.109375 to 0.109375
- rel_bias: float32 [320, 24], P(None, 'tp'), may hold values from -5 to 254
- d_out: bfloat16 [16384, 1536], P('sp', 'tp'), may hold values from -6 to 6
Outputs:
- grad_inputs: bfloat16 [16384, 3072], P('sp', 'tp')
- grad_w_query: float32 [3072, 1536], P('sp', 'tp')
- grad_w_key: float32 [3072, 1536], P('sp', 'tp')
- grad_w_value: float32 [3072, 1536], P('sp', 'tp')
- grad_bias: float32 [320, 24], P(None, 'tp')
All inputs are finite; a program needn't handle non-finite values.
Results may differ from a plain program's by a relative error of at most 0.015.
Values may be sent and summed in bfloat16 or wider, within the bound.
A program may use at most 128 MiB of HBM per device.

v0:
```python
import functools

import jax
import jax.numpy as jnp
from jax import lax
from jax.experimental import pallas as pl
from jax.experimental.pallas import tpu as pltpu
from jax.sharding import Mesh
from jax.sharding import PartitionSpec as P

SP = ("sp_0", "sp_1", "sp_2")
MESH = pl.DeviceIdType.MESH
BF = jnp.bfloat16
F32 = jnp.float32
NSEM = 100

NN = (((1,), (0,)), ((), ()))
NT = (((1,), (1,)), ((), ()))


def dot(a, b, dims=NN):
    return lax.dot_general(a, b, dims, preferred_element_type=F32)


def kernel(
    x_hbm, wq_hbm, wk_hbm, wv_hbm, rb_hbm, do_hbm,
    gx_ref, gw_ref, gb_ref,
    xbuf, w, xt, acc, kext, vext, qs, do, kt, dk_acc, dv_acc, bias, gbias, g,
    hb_send, hb_recv, dwb, crecv, s1,
    fold, recv2, s2, recv3,
    dx_send, dx_fold, dx_recv, dx_part, dx_own,
    rbuf, gl, gl_c, gl_s, gl_y, gl_z,
    lsem_x, lsem_b, lsem_w, lsem_do, ssem, rsem,
):
    x = lax.axis_index("tp")
    z = lax.axis_index("sp_0")
    y = lax.axis_index("sp_1")
    c = lax.axis_index("sp_2")
    spi = (z * 4 + y) * 2 + c
    right = {"tp": (x + 1) % 4}
    left = {"tp": (x + 3) % 4}
    nxt = (spi + 1) % 32
    prv = (spi + 31) % 32
    sp_next = {"sp_0": nxt // 8, "sp_1": (nxt // 2) % 4, "sp_2": nxt % 2}
    sp_prev = {"sp_0": prv // 8, "sp_1": (prv // 2) % 4, "sp_2": prv % 2}
    partner = {"sp_2": 1 - c}
    ydev = [None] + [{"sp_1": (y + r) % 4} for r in (1, 2, 3)]
    zdev = [None] + [{"sp_0": (z + r) % 4} for r in (1, 2, 3)]
    yid = [(y + r) % 4 for r in range(4)]
    zid = [(z + r) % 4 for r in range(4)]
    src = [x, (x + 3) % 4, (x + 1) % 4, (x + 2) % 4]

    counter = [0]
    started = []

    def send(src_ref, dst_ref, dev):
        i = counter[0]
        counter[0] += 1
        cp = pltpu.make_async_remote_copy(
            src_ref=src_ref, dst_ref=dst_ref, send_sem=ssem.at[i], recv_sem=rsem.at[i],
            device_id=dev, device_id_type=MESH,
        )
        cp.start()
        started.append(cp)
        return cp

    x_copy = pltpu.make_async_copy(x_hbm, xbuf.at[:, pl.ds(0, 768)], lsem_x)
    x_copy.start()
    barrier = pltpu.get_barrier_semaphore()
    peers = [left, right, partner, sp_next, sp_prev] + ydev[1:] + zdev[1:]
    for dev in peers:
        pl.semaphore_signal(barrier, inc=1, device_id=dev, device_id_type=MESH)
    b_copy = pltpu.make_async_copy(rb_hbm, rbuf, lsem_b)
    gl[...] = jnp.zeros_like(gl)
    b_copy.start()
    x_copy.wait()
    pl.semaphore_wait(barrier, len(peers))

    order = (3, 2, 1, 0)
    from_left, from_right, opp_a, opp_b = {}, {}, {}, {}
    slot = [pl.ds(768 * i, 768) for i in range(4)]

    def send_own(j):
        rows = pl.ds(128 * j, 128)
        from_left[j] = send(xbuf.at[rows, slot[0]], xbuf.at[rows, slot[1]], right)
        from_right[j] = send(xbuf.at[rows, slot[0]], xbuf.at[rows, slot[2]], left)

    def forward(j):
        first, second = pl.ds(128 * j, 64), pl.ds(128 * j + 64, 64)
        from_left[j].wait_recv()
        opp_a[j] = send(xbuf.at[first, slot[1]], xbuf.at[first, slot[3]], right)
        from_right[j].wait_recv()
        opp_b[j] = send(xbuf.at[second, slot[2]], xbuf.at[second, slot[3]], left)

    def project_a(j):
        rows = pl.ds(128 * j, 128)

        def body(hp, carry):
            cols = pl.ds(pl.multiple_of(hp * 384, 128), 384)
            acc[j % 2, hp] = dot(xbuf[rows, 0:2304], w[0:2304, cols])
            return carry

        lax.fori_loop(0, 3, body, 0)

    def project_b(j):
        opp_a[j].wait_recv()
        opp_b[j].wait_recv()
        rows = pl.ds(128 * j, 128)
        ext = pl.ds(256 + 128 * j, 128)

        def body(hp, carry):
            cols = pl.ds(pl.multiple_of(hp * 384, 128), 384)
            out = (acc[j % 2, hp] + dot(xbuf[rows, 2304:3072], w[2304:3072, cols])).astype(BF)
            qs[hp, rows] = out[:, :128] * jnp.asarray(0.125, BF)
            kext[hp, ext] = out[:, 128:256]
            kt[hp, :, ext] = out[:, 128:256].T
            vext[hp, ext] = out[:, 256:]
            return carry

        lax.fori_loop(0, 3, body, 0)

    def transpose_rows(j):
        rows = pl.ds(128 * j, 128)
        for s in range(4):
            xt[src[s], :, rows] = xbuf[rows, slot[s]].T

    send_own(order[0])
    send_own(order[1])

    w_copies = []
    for s in range(4):
        for hp in range(3):
            for m, ref in enumerate((wq_hbm, wk_hbm, wv_hbm)):
                cp = pltpu.make_async_copy(
                    ref.at[pl.ds(src[s] * 768, 768), pl.ds(128 * hp, 128)],
                    w.at[slot[s], pl.ds(384 * hp + 128 * m, 128)],
                    lsem_w.at[(hp * 4 + s) * 3 + m],
                )
                cp.start()
                w_copies.append(cp)
    do_copies = []
    for hp in range(3):
        cp = pltpu.make_async_copy(do_hbm.at[:, pl.ds(128 * hp, 128)], do.at[hp], lsem_do.at[hp])
        cp.start()
        do_copies.append(cp)

    b_copy.wait()
    gl[0:6, 0:320] = rbuf[...]
    line = pltpu.roll(gl[...], 193, 1)
    lane = lax.broadcasted_iota(jnp.int32, (8, 512), 1)
    line = jnp.where((lane > 0) & (lane < 128), line[:, 0:1], line)
    gl[...] = line
    key_seg = lax.broadcasted_iota(jnp.int32, (384, 128), 0) // 64
    query_seg = lax.broadcasted_iota(jnp.int32, (384, 128), 1) // 64
    seen = (key_seg >= query_seg) & (key_seg <= query_seg + 4)
    for h in range(6):
        wide = jnp.broadcast_to(gl[h : h + 1, :], (384, 512))
        wide = pltpu.roll(wide, 0, 1, stride=1, stride_axis=0)
        bias[h // 2, :, pl.ds(128 * (h % 2), 128)] = jnp.where(seen, wide[:, :128], -jnp.inf)
    gbias[...] = jnp.zeros_like(gbias)
    dk_acc[...] = jnp.zeros_like(dk_acc)
    dv_acc[...] = jnp.zeros_like(dv_acc)

    for cp in w_copies + do_copies:
        cp.wait()

    forward(order[0])
    send_own(order[2])
    project_a(order[0])
    forward(order[1])
    send_own(order[3])
    project_a(order[1])
    project_b(order[0])
    transpose_rows(order[0])
    forward(order[2])
    project_a(order[2])
    project_b(order[1])
    halo_k = send(kext.at[:, pl.ds(512, 256)], kext.at[:, pl.ds(0, 256)], sp_next)
    halo_v = send(vext.at[:, pl.ds(512, 256)], vext.at[:, pl.ds(0, 256)], sp_next)
    transpose_rows(order[1])
    forward(order[3])
    project_a(order[3])
    project_b(order[2])

    lane_q = lax.broadcasted_iota(jnp.int32, (128, 128), 1)
    row_f = lax.broadcasted_iota(jnp.int32, (128, 128), 0)
    zero = jnp.zeros((128, 128), BF)

    def stacked(block):
        return jnp.concatenate(
            [jnp.where(lane_q < 64, block, zero), jnp.where(lane_q >= 64, block, zero)], axis=0
        )

    pen = jnp.where(spi == 0, -jnp.inf, 0.0).astype(F32)

    def unit(hp, qp):
        rows = pl.ds(qp * 128, 128)
        keys = pl.ds(qp * 128, 384)
        qm = stacked(qs[hp, rows])
        dm = stacked(do[hp, rows])
        score = dot(kext[hp, keys], qm, NT) + bias[hp]
        if qp < 2:
            cut = 256 - 128 * qp
            score = jnp.concatenate([score[:cut] + pen, score[cut:]], axis=0)
        top = jnp.max(score, axis=0, keepdims=True)
        e = jnp.exp(score - top)
        inv = 1.0 / jnp.sum(e, axis=0, keepdims=True)
        prob = e * inv
        low = prob.astype(BF)
        gp = dot(vext[hp, keys], dm, NT)
        delta = jnp.sum(low.astype(F32) * gp, axis=0, keepdims=True)
        ds = prob * (gp - delta)
        gbias[hp] += ds
        dlow = ds.astype(BF)
        dk_acc[hp, keys] += dot(dlow, qm)
        dv_acc[hp, keys] += dot(low, dm)
        dqt = dot(kt[hp, :, keys], dlow)
        dqt = jnp.where(row_f < 64, dqt[:, :128], dqt[:, 128:]) * 0.125
        g[rows, pl.ds(384 * hp, 128)] = dqt.T.astype(BF)

    def last_units():
        for hp in range(3):
            unit(hp, 3)

    last_units()
    project_b(order[3])
    halo_k.wait_recv()
    halo_v.wait_recv()
    for hp in range(3):
        kt[hp, :, 0:256] = kext[hp, 0:256].T

    halo_back = {}

    def attention(hp):
        unit(hp, 0)
        unit(hp, 1)
        hb_send[hp, 0] = dk_acc[hp, 0:256].astype(BF)
        hb_send[hp, 1] = dv_acc[hp, 0:256].astype(BF)
        halo_back[hp] = send(hb_send.at[hp], hb_recv.at[hp], sp_prev)
        unit(hp, 2)
        g[0:256, pl.ds(384 * hp + 128, 128)] = dk_acc[hp, 256:512].astype(BF)
        g[0:256, pl.ds(384 * hp + 256, 128)] = dv_acc[hp, 256:512].astype(BF)

    def finish_grads(hp):
        halo_back[hp].wait_recv()
        g[256:512, pl.ds(384 * hp + 128, 128)] = (
            dk_acc[hp, 512:768] + hb_recv[hp, 0].astype(F32)
        ).astype(BF)
        g[256:512, pl.ds(384 * hp + 256, 128)] = (
            dv_acc[hp, 512:768] + hb_recv[hp, 1].astype(F32)
        ).astype(BF)

    core_copy = {}

    def weight_grad(hp):
        def body(i, carry):
            out = dot(xt[i], g[:, 384 * hp : 384 * hp + 384]).astype(BF)
            dwb[hp, pl.ds(4 * i, 4)] = out.reshape(4, 2, 96, 384)
            return carry

        lax.fori_loop(0, 4, body, 0)
        core_copy[hp] = send(dwb.at[hp, :, 1 - c], crecv.at[hp], partner)

    lo, hi = pl.ds(0, 2), pl.ds(2, 2)
    ra, rb = pl.ds(0, 48), pl.ds(48, 48)
    st2 = {}

    def rs_start(hp):
        core_copy[hp].wait_recv()

        def body(i, carry):
            zz, yy = i // 4, i % 4
            s1[hp, zz, yy] = (dwb[hp, i, c].astype(F32) + crecv[hp, i].astype(F32)).astype(BF)
            return carry

        lax.fori_loop(0, 16, body, 0)
        f = {}
        f["ra"] = send(s1.at[hp, lo, yid[2], ra], fold.at[hp, 0], ydev[1])
        f["la"] = send(s1.at[hp, hi, yid[2], ra], fold.at[hp, 1], ydev[3])
        f["rb"] = send(s1.at[hp, zid[2], lo, rb], fold.at[hp, 2], zdev[1])
        f["lb"] = send(s1.at[hp, zid[2], hi, rb], fold.at[hp, 3], zdev[3])
        f["ura"] = send(s1.at[hp, hi, yid[1], ra], recv2.at[hp, 0, hi], ydev[1])
        f["ula"] = send(s1.at[hp, lo, yid[3], ra], recv2.at[hp, 1, lo], ydev[3])
        f["urb"] = send(s1.at[hp, zid[1], hi, rb], recv2.at[hp, 2, hi], zdev[1])
        f["ulb"] = send(s1.at[hp, zid[3], lo, rb], recv2.at[hp, 3, lo], zdev[3])
        st2[hp] = f

    def rs_fold(hp):
        f = st2[hp]

        def add(k, index):
            for i in range(2):
                at = index(i)
                s1[at] = (s1[at].astype(F32) + fold[hp, k, i].astype(F32)).astype(BF)

        f["ra"].wait_recv()
        add(0, lambda i: (hp, i, yid[1], ra))
        f["fra"] = send(s1.at[hp, lo, yid[1], ra], recv2.at[hp, 0, lo], ydev[1])
        f["la"].wait_recv()
        add(1, lambda i: (hp, 2 + i, yid[3], ra))
        f["fla"] = send(s1.at[hp, hi, yid[3], ra], recv2.at[hp, 1, hi], ydev[3])
        f["rb"].wait_recv()
        add(2, lambda i: (hp, zid[1], i, rb))
        f["frb"] = send(s1.at[hp, zid[1], lo, rb], recv2.at[hp, 2, lo], zdev[1])
        f["lb"].wait_recv()
        add(3, lambda i: (hp, zid[3], 2 + i, rb))
        f["flb"] = send(s1.at[hp, zid[3], hi, rb], recv2.at[hp, 3, hi], zdev[3])

    st3 = {}

    def rs_second(hp):
        f = st2[hp]
        for k in ("ura", "ula", "urb", "ulb", "fra", "fla", "frb", "flb"):
            f[k].wait_recv()
        for i in range(4):
            s2[hp, 0, i] = (
                s1[hp, i, y, ra].astype(F32)
                + recv2[hp, 0, i].astype(F32)
                + recv2[hp, 1, i].astype(F32)
            ).astype(BF)
            s2[hp, 1, i] = (
                s1[hp, z, i, rb].astype(F32)
                + recv2[hp, 2, i].astype(F32)
                + recv2[hp, 3, i].astype(F32)
            ).astype(BF)
        st3[hp] = [send(s2.at[hp, 0, zid[r]], recv3.at[hp, 0, r - 1], zdev[r]) for r in (1, 3, 2)]
        st3[hp] += [send(s2.at[hp, 1, yid[r]], recv3.at[hp, 1, r - 1], ydev[r]) for r in (1, 3, 2)]

    def rs_finish(hp):
        for cp in st3[hp]:
            cp.wait_recv()
        cols = pl.ds(128 * hp, 128)
        for part, own in ((0, z), (1, y)):
            total = s2[hp, part, own].astype(F32)
            for r in range(3):
                total += recv3[hp, part, r].astype(F32)
            rows = pl.ds(48 * part, 48)
            for m in range(3):
                gw_ref[m, rows, cols] = total[:, 128 * m : 128 * m + 128]

    def dx_block(t, s):
        return dot(w[slot[s], :], g[256 * t : 256 * t + 256, :], NT)

    dxc = {}
    half_a, half_b = pl.ds(0, 384), pl.ds(384, 384)

    def dx_opposite(t):
        out = dx_block(t, 3).astype(BF)
        dx_send[t, 0] = out[:384]
        dx_send[t, 1] = out[384:]
        dxc[t, "fr"] = send(dx_send.at[t, 0], dx_fold.at[t, 0], right)
        dxc[t, "fl"] = send(dx_send.at[t, 1], dx_fold.at[t, 1], left)

    def dx_direct(t):
        out = dx_block(t, 2)
        dx_send[t, 2] = out[384:].astype(BF)
        dxc[t, "ur"] = send(dx_send.at[t, 2], dx_recv.at[t, 0, half_b], right)
        dx_part[t, 0] = out[:384]
        out = dx_block(t, 1)
        dx_send[t, 3] = out[:384].astype(BF)
        dxc[t, "ul"] = send(dx_send.at[t, 3], dx_recv.at[t, 1, half_a], left)
        dx_part[t, 1] = out[384:]

    def dx_folded(t):
        dxc[t, "fr"].wait_recv()
        dx_send[t, 4] = (dx_part[t, 0] + dx_fold[t, 0].astype(F32)).astype(BF)
        dxc[t, "gr"] = send(dx_send.at[t, 4], dx_recv.at[t, 0, half_a], right)
        dxc[t, "fl"].wait_recv()
        dx_send[t, 5] = (dx_part[t, 1] + dx_fold[t, 1].astype(F32)).astype(BF)
        dxc[t, "gl"] = send(dx_send.at[t, 5], dx_recv.at[t, 1, half_b], left)

    def dx_mine(t):
        dx_own[t] = dx_block(t, 0)

    def dx_finish(t):
        for half, names in ((1, ("ur", "gl")), (0, ("ul", "gr"))):
            for k in names:
                dxc[t, k].wait_recv()
            rows = pl.ds(384 * half, 384)
            total = (
                dx_own[t, rows] + dx_recv[t, 0, rows].astype(F32) + dx_recv[t, 1, rows].astype(F32)
            )
            gx_ref[pl.ds(256 * t, 256), rows] = total.T.astype(BF)

    def bias_line():
        for hp in range(3):
            for par in range(2):
                total = jnp.zeros((8, 512), F32)
                for a in range(48):
                    part = gbias[hp, pl.ds(8 * a, 8), pl.ds(128 * par, 128)]
                    part = jnp.concatenate([part, jnp.zeros((8, 384), F32)], axis=1)
                    total += pltpu.roll(part, (512 - 8 * a) % 512, 1)
                sub = lax.broadcasted_iota(jnp.int32, (8, 512), 0)
                for bit in range(3):
                    moved = pltpu.roll(total, 512 - (1 << bit), 1)
                    total = jnp.where((sub >> bit) % 2 == 1, moved, total)
                h = 2 * hp + par
                gl[h : h + 1, :] = jnp.sum(total, axis=0, keepdims=True)
        gl[6:8, :] = jnp.zeros((2, 512), F32)

    attention(0)
    attention(1)
    attention(2)
    dx_opposite(0)
    dx_direct(0)
    transpose_rows(order[2])
    transpose_rows(order[3])
    finish_grads(0)
    weight_grad(0)
    finish_grads(1)
    finish_grads(2)
    dx_opposite(1)
    dx_direct(1)
    rs_start(0)
    weight_grad(1)
    dx_folded(0)
    rs_fold(0)
    weight_grad(2)
    rs_start(1)
    bias_line()
    gbc = send(gl, gl_c, partner)
    rs_second(0)
    rs_fold(1)
    rs_start(2)
    dx_folded(1)
    gbc.wait_recv()
    gl_s[0] = gl[...] + gl_c[...]
    gby = [send(gl_s.at[0], gl_y.at[r - 1], ydev[r]) for r in (1, 2, 3)]
    dx_mine(0)
    rs_second(1)
    rs_fold(2)
    dx_mine(1)
    rs_finish(0)
    for cp in gby:
        cp.wait_recv()
    gl_s[1] = gl_s[0] + gl_y[0] + gl_y[1] + gl_y[2]
    gbz = [send(gl_s.at[1], gl_z.at[r - 1], zdev[r]) for r in (1, 2, 3)]
    rs_second(2)
    rs_finish(1)
    dx_finish(0)
    for cp in gbz:
        cp.wait_recv()
    total = gl_s[1] + gl_z[0] + gl_z[1] + gl_z[2]
    far = jnp.sum(jnp.where(lane < 128, total, 0.0), axis=1, keepdims=True)
    total = jnp.where(lane == 0, far, total)
    total = pltpu.roll(total, 512 - 193, 1)
    gb_ref[...] = total[0:6, 0:320]
    rs_finish(2)
    dx_finish(1)
    for cp in started:
        cp.wait_send()


def write_out(gx, gw, gb, gx_out, gwq_out, gwk_out, gwv_out, gb_out, sem):
    pairs = [(gx, gx_out), (gw.at[0], gwq_out), (gw.at[1], gwk_out), (gw.at[2], gwv_out), (gb, gb_out)]
    copies = [pltpu.make_async_copy(a, b, sem.at[i]) for i, (a, b) in enumerate(pairs)]
    for cp in copies:
        cp.start()
    for cp in copies:
        cp.wait()


def local(inputs, w_query, w_key, w_value, rel_bias, d_out):
    any_spec = pl.BlockSpec(memory_space=pl.ANY)
    vmem = pl.BlockSpec(memory_space=pltpu.VMEM)
    V = pltpu.VMEM
    gx, gw, gb = pl.pallas_call(
        kernel,
        out_shape=(V((512, 768), BF), V((3, 96, 384), F32), V((6, 320), F32)),
        in_specs=[any_spec] * 6,
        out_specs=(vmem, vmem, vmem),
        scratch_shapes=[
            V((512, 3072), BF),
            V((3072, 1152), BF),
            V((4, 768, 512), BF),
            V((2, 3, 128, 384), F32),
            V((3, 768, 128), BF),
            V((3, 768, 128), BF),
            V((3, 512, 128), BF),
            V((3, 512, 128), BF),
            V((3, 128, 768), BF),
            V((3, 768, 128), F32),
            V((3, 768, 128), F32),
            V((3, 384, 256), F32),
            V((3, 384, 256), F32),
            V((512, 1152), BF),
            V((3, 2, 256, 128), BF),
            V((3, 2, 256, 128), BF),
            V((3, 16, 2, 96, 384), BF),
            V((3, 16, 96, 384), BF),
            V((3, 4, 4, 96, 384), BF),
            V((3, 4, 2, 48, 384), BF),
            V((3, 4, 4, 48, 384), BF),
            V((3, 2, 4, 48, 384), BF),
            V((3, 2, 3, 48, 384), BF),
            V((2, 6, 384, 256), BF),
            V((2, 2, 384, 256), BF),
            V((2, 2, 768, 256), BF),
            V((2, 2, 384, 256), F32),
            V((2, 768, 256), F32),
            V((6, 320), F32),
            V((8, 512), F32),
            V((8, 512), F32),
            V((2, 8, 512), F32),
            V((3, 8, 512), F32),
            V((3, 8, 512), F32),
            pltpu.SemaphoreType.DMA,
            pltpu.SemaphoreType.DMA,
            pltpu.SemaphoreType.DMA((36,)),
            pltpu.SemaphoreType.DMA((3,)),
            pltpu.SemaphoreType.DMA((NSEM,)),
            pltpu.SemaphoreType.DMA((NSEM,)),
        ],
        compiler_params=pltpu.CompilerParams(
            collective_id=0, has_side_effects=True, vmem_limit_bytes=58 * 1024 * 1024
        ),
    )(inputs, w_query, w_key, w_value, rel_bias.T, d_out)
    gx, gwq, gwk, gwv, gb = pl.pallas_call(
        write_out,
        out_shape=(
            jax.ShapeDtypeStruct((512, 768), BF),
            jax.ShapeDtypeStruct((96, 384), F32),
            jax.ShapeDtypeStruct((96, 384), F32),
            jax.ShapeDtypeStruct((96, 384), F32),
            jax.ShapeDtypeStruct((6, 320), F32),
        ),
        in_specs=[vmem] * 3,
        out_specs=[any_spec] * 5,
        scratch_shapes=[pltpu.SemaphoreType.DMA((5,))],
        compiler_params=pltpu.CompilerParams(vmem_limit_bytes=4 * 1024 * 1024),
    )(gx, gw, gb)
    return gx, gwq, gwk, gwv, gb.T


def solution(mesh):
    torus = Mesh(mesh.devices.reshape(4, 4, 2, mesh.shape["tp"]), ("sp_0", "sp_1", "sp_2", "tp"))
    return jax.shard_map(
        local,
        mesh=torus,
        in_specs=(
            P(SP, "tp"),
            P(None, "tp"),
            P(None, "tp"),
            P(None, "tp"),
            P(None, "tp"),
            P(SP, "tp"),
        ),
        out_specs=(P(SP, "tp"), P(SP, "tp"), P(SP, "tp"), P(SP, "tp"), P(None, "tp")),
        check_vma=False,
    )
```

profile of v0, /device:TPU:0, one launch (start us, length us, event | category | flops | bytes accessed | tf_op | source)
XLA Modules:
  0.0 83.5 jit_solution(9357928660271599874)
XLA Ops:
  0.6 81.7 %shard_map.101 = (bf16[512,768]{1,0:T(8,128)(2,1)S(1)}, f32[3,96,384]{2,1,0:T(8,128)S(1)}, f32[6,320]{1,0:T(8,128)S(1)}) custom-call(bf16[512,768]{1,0:T(8,128)(2,1)} %x_hbm.1, bf16[3072,384]{1,0:T(8,128)(2,1)} %wq_hbm.1, bf16[3072,384]{1,0:T(8,128)(2,1)} %wk_hbm.1, bf16[3072,384]{1,0:T(8,128)(2,1)} %wv_hbm.1, f32[6,320]{1,0:T(8,128)} %bitcast.2, ...), custom_call_target="tpu_custom_call" | custom-call | tf_op jit(solution)/shard_map/pallas_call | solution.py:467
  82.3 1.1 %shard_map.102 = (bf16[512,768]{1,0:T(8,128)(2,1)}, f32[96,384]{1,0:T(8,128)}, f32[96,384]{1,0:T(8,128)}, f32[96,384]{1,0:T(8,128)}, f32[6,320]{1,0:T(8,128)}) custom-call(bf16[512,768]{1,0:T(8,128)(2,1)S(1)} %get-tuple-element.13.gx, f32[3,96,384]{2,1,0:T(8,128)S(1)} %get-tuple-element.14.gw, f32[6,320]{1,0:T(8,128)S(1)} %get-tuple-element.15.gb), custom_call_target="tpu_custom_call" | custom-call | tf_op jit(solution)/shard_map/pallas_call | solution.py:518
where the time goes:
time: 83.7 us; the launch traced here: 83.5 us
  Pallas kernels  82.7 us (99%)
    pallas_call x1, Pallas kernels, local(): pl.pallas_call(kernel, out_shape=(V((512, 768), BF), V((3, 96, 384), F32)...  81.7 us

commit v1 on v0

v1 whole, which is shorter than its diff:
```python
import functools

import jax
import jax.numpy as jnp
from jax import lax
from jax.experimental import pallas as pl
from jax.experimental.pallas import tpu as pltpu
from jax.sharding import Mesh
from jax.sharding import PartitionSpec as P

SP = ("sp_0", "sp_1", "sp_2")
MESH = pl.DeviceIdType.MESH
BF = jnp.bfloat16
F32 = jnp.float32
SENDS, RECVS = 10, 36

NN = (((1,), (0,)), ((), ()))
NT = (((1,), (1,)), ((), ()))


def dot(a, b, dims=NN):
    return lax.dot_general(a, b, dims, preferred_element_type=F32)


def kernel(
    x_hbm, wq_hbm, wk_hbm, wv_hbm, rb_hbm, do_hbm,
    gx_ref, gw_ref, gb_ref,
    xbuf, w, xt, acc, kext, vext, qs, do, kt, dk_acc, dv_acc, bias, gbias, g,
    hb_send, hb_recv, dwb, crecv, s1,
    fold, recv2, s2, recv3,
    dx_send, dx_fold, dx_recv, dx_part, dx_own,
    rbuf, gl, gl_c, gl_s, gl_r,
    lsem_x, lsem_b, lsem_w, lsem_do, ssem, rsem,
):
    x = lax.axis_index("tp")
    z = lax.axis_index("sp_0")
    y = lax.axis_index("sp_1")
    c = lax.axis_index("sp_2")
    spi = (z * 4 + y) * 2 + c
    right = {"tp": (x + 1) % 4}
    left = {"tp": (x + 3) % 4}
    nxt = (spi + 1) % 32
    prv = (spi + 31) % 32
    sp_next = {"sp_0": nxt // 8, "sp_1": (nxt // 2) % 4, "sp_2": nxt % 2}
    sp_prev = {"sp_0": prv // 8, "sp_1": (prv // 2) % 4, "sp_2": prv % 2}
    partner = {"sp_2": 1 - c}
    ydev = [None] + [{"sp_1": (y + r) % 4} for r in (1, 2, 3)]
    zdev = [None] + [{"sp_0": (z + r) % 4} for r in (1, 2, 3)]
    yid = [(y + r) % 4 for r in range(4)]
    zid = [(z + r) % 4 for r in range(4)]
    src = [x, (x + 3) % 4, (x + 1) % 4, (x + 2) % 4]

    sends, recvs = {}, {}

    def send(src_ref, dst_ref, dev, out, back):
        pltpu.make_async_remote_copy(
            src_ref=src_ref, dst_ref=dst_ref,
            send_sem=ssem.at[sends.setdefault(out, len(sends))],
            recv_sem=rsem.at[recvs.setdefault(back, len(recvs))],
            device_id=dev, device_id_type=MESH,
        ).start()

    def arrived(back, ref):
        pltpu.make_async_copy(ref, ref, rsem.at[recvs[back]]).wait()

    def sent(out, ref):
        pltpu.make_async_copy(ref, ref, ssem.at[sends[out]]).wait()

    x_copy = pltpu.make_async_copy(x_hbm, xbuf.at[:, pl.ds(0, 768)], lsem_x)
    x_copy.start()
    barrier = pltpu.get_barrier_semaphore()
    peers = [left, right, partner, sp_next, sp_prev] + ydev[1:] + zdev[1:]
    for dev in peers:
        pl.semaphore_signal(barrier, inc=1, device_id=dev, device_id_type=MESH)
    b_copy = pltpu.make_async_copy(rb_hbm, rbuf, lsem_b)
    gl[...] = jnp.zeros_like(gl)
    b_copy.start()
    x_copy.wait()
    pl.semaphore_wait(barrier, len(peers))

    order = (3, 2, 1, 0)
    slot = [pl.ds(768 * i, 768) for i in range(4)]

    def send_own(j):
        rows = pl.ds(128 * j, 128)
        send(xbuf.at[rows, slot[0]], xbuf.at[rows, slot[1]], right, "x", ("xl", j))
        send(xbuf.at[rows, slot[0]], xbuf.at[rows, slot[2]], left, "x", ("xr", j))

    def forward(j):
        rows, first, second = pl.ds(128 * j, 128), pl.ds(128 * j, 64), pl.ds(128 * j + 64, 64)
        arrived(("xl", j), xbuf.at[rows, slot[1]])
        send(xbuf.at[first, slot[1]], xbuf.at[first, slot[3]], right, "x", ("xo", j))
        arrived(("xr", j), xbuf.at[rows, slot[2]])
        send(xbuf.at[second, slot[2]], xbuf.at[second, slot[3]], left, "x", ("xo", j))

    def project_a(j):
        rows = pl.ds(128 * j, 128)

        def body(m, carry):
            cols = pl.ds(pl.multiple_of(m * 384, 128), 384)
            acc[j % 2, m] = dot(xbuf[rows, 0:2304], w[0:2304, cols])
            return carry

        lax.fori_loop(0, 3, body, 0)

    def project_b(j):
        rows = pl.ds(128 * j, 128)
        ext = pl.ds(256 + 128 * j, 128)
        arrived(("xo", j), xbuf.at[rows, slot[3]])
        for m in range(3):
            out = acc[j % 2, m] + dot(xbuf[rows, 2304:3072], w[2304:3072, 384 * m : 384 * m + 384])
            out = out.astype(BF)
            for hp in range(3):
                one = out[:, 128 * hp : 128 * hp + 128]
                if m == 0:
                    qs[hp, rows] = one * jnp.asarray(0.125, BF)
                elif m == 1:
                    kext[hp, ext] = one
                    kt[hp, :, ext] = one.T
                else:
                    vext[hp, ext] = one

    def transpose_rows(j):
        rows = pl.ds(128 * j, 128)
        for s in range(4):
            xt[src[s], :, rows] = xbuf[rows, slot[s]].T

    send_own(order[0])
    send_own(order[1])

    for i in range(4):
        for m, ref in enumerate((wq_hbm, wk_hbm, wv_hbm)):
            pltpu.make_async_copy(
                ref.at[pl.ds(src[i] * 768, 768)], w.at[slot[i], pl.ds(384 * m, 384)], lsem_w
            ).start()
    do_copy = pltpu.make_async_copy(do_hbm, do, lsem_do)
    do_copy.start()

    b_copy.wait()
    gl[0:6, 0:320] = rbuf[...]
    line = pltpu.roll(gl[...], 193, 1)
    lane = lax.broadcasted_iota(jnp.int32, (8, 512), 1)
    line = jnp.where((lane > 0) & (lane < 128), line[:, 0:1], line)
    gl[...] = line
    key_seg = lax.broadcasted_iota(jnp.int32, (384, 128), 0) // 64
    query_seg = lax.broadcasted_iota(jnp.int32, (384, 128), 1) // 64
    seen = (key_seg >= query_seg) & (key_seg <= query_seg + 4)
    for h in range(6):
        wide = jnp.broadcast_to(gl[h : h + 1, :], (384, 512))
        wide = pltpu.roll(wide, 0, 1, stride=1, stride_axis=0)
        bias[h // 2, :, pl.ds(128 * (h % 2), 128)] = jnp.where(seen, wide[:, :128], -jnp.inf)
    gbias[...] = jnp.zeros_like(gbias)
    dk_acc[...] = jnp.zeros_like(dk_acc)
    dv_acc[...] = jnp.zeros_like(dv_acc)

    pltpu.make_async_copy(w, w, lsem_w).wait()
    do_copy.wait()

    forward(order[0])
    send_own(order[2])
    project_a(order[0])
    forward(order[1])
    send_own(order[3])
    project_a(order[1])
    project_b(order[0])
    transpose_rows(order[0])
    forward(order[2])
    project_a(order[2])
    project_b(order[1])
    send(kext.at[:, pl.ds(512, 256)], kext.at[:, pl.ds(0, 256)], sp_next, "h", "hk")
    send(vext.at[:, pl.ds(512, 256)], vext.at[:, pl.ds(0, 256)], sp_next, "h", "hv")
    transpose_rows(order[1])
    forward(order[3])
    project_a(order[3])
    project_b(order[2])

    lane_q = lax.broadcasted_iota(jnp.int32, (128, 128), 1)
    row_f = lax.broadcasted_iota(jnp.int32, (128, 128), 0)
    zero = jnp.zeros((128, 128), BF)

    def stacked(block):
        return jnp.concatenate(
            [jnp.where(lane_q < 64, block, zero), jnp.where(lane_q >= 64, block, zero)], axis=0
        )

    pen = jnp.where(spi == 0, -jnp.inf, 0.0).astype(F32)

    def unit(hp, qp):
        rows = pl.ds(qp * 128, 128)
        keys = pl.ds(qp * 128, 384)
        qm = stacked(qs[hp, rows])
        dm = stacked(do[rows, 128 * hp : 128 * hp + 128])
        score = dot(kext[hp, keys], qm, NT) + bias[hp]
        if qp < 2:
            cut = 256 - 128 * qp
            score = jnp.concatenate([score[:cut] + pen, score[cut:]], axis=0)
        top = jnp.max(score, axis=0, keepdims=True)
        e = jnp.exp(score - top)
        inv = 1.0 / jnp.sum(e, axis=0, keepdims=True)
        prob = e * inv
        low = prob.astype(BF)
        gp = dot(vext[hp, keys], dm, NT)
        delta = jnp.sum(prob * gp, axis=0, keepdims=True)
        ds = prob * (gp - delta)
        gbias[hp] += ds
        dlow = ds.astype(BF)
        dk_acc[hp, keys] += dot(dlow, qm)
        dv_acc[hp, keys] += dot(low, dm)
        dqt = dot(kt[hp, :, keys], dlow)
        dqt = jnp.where(row_f < 64, dqt[:, :128], dqt[:, 128:]) * 0.125
        g[rows, pl.ds(128 * hp, 128)] = dqt.T.astype(BF)

    def last_units():
        for hp in range(3):
            unit(hp, 3)

    last_units()
    project_b(order[3])
    arrived("hk", kext.at[:, pl.ds(0, 256)])
    arrived("hv", vext.at[:, pl.ds(0, 256)])
    for hp in range(3):
        kt[hp, :, 0:256] = kext[hp, 0:256].T

    def attention():
        for hp in range(3):
            unit(hp, 0)
            unit(hp, 1)
        for hp in range(3):
            hb_send[hp, 0] = dk_acc[hp, 0:256].astype(BF)
            hb_send[hp, 1] = dv_acc[hp, 0:256].astype(BF)
        for hp in range(3):
            send(hb_send.at[hp], hb_recv.at[hp], sp_prev, "hb", ("hb", hp))
        for hp in range(3):
            unit(hp, 2)
        for hp in range(3):
            g[0:256, pl.ds(384 + 128 * hp, 128)] = dk_acc[hp, 256:512].astype(BF)
            g[0:256, pl.ds(768 + 128 * hp, 128)] = dv_acc[hp, 256:512].astype(BF)

    def finish_grads(hp):
        arrived(("hb", hp), hb_recv.at[hp])
        g[256:512, pl.ds(384 + 128 * hp, 128)] = (
            dk_acc[hp, 512:768] + hb_recv[hp, 0].astype(F32)
        ).astype(BF)
        g[256:512, pl.ds(768 + 128 * hp, 128)] = (
            dv_acc[hp, 512:768] + hb_recv[hp, 1].astype(F32)
        ).astype(BF)

    def weight_grad(hp):
        def body(i, carry):
            grads = jnp.concatenate(
                [g[:, 384 * m + 128 * hp : 384 * m + 128 * hp + 128] for m in range(3)], axis=1
            )
            out = dot(xt[i], grads).astype(BF)
            dwb[hp, pl.ds(4 * i, 4)] = out.reshape(4, 2, 96, 384)
            return carry

        lax.fori_loop(0, 4, body, 0)
        send(dwb.at[hp, :, 1 - c], crecv.at[hp], partner, "c", ("c", hp))

    lo, hi = pl.ds(0, 2), pl.ds(2, 2)
    ra, rb = pl.ds(0, 48), pl.ds(48, 48)

    def rs_start(hp):
        arrived(("c", hp), crecv.at[hp])

        def body(i, carry):
            zz, yy = i // 4, i % 4
            s1[hp, zz, yy] = (dwb[hp, i, c].astype(F32) + crecv[hp, i].astype(F32)).astype(BF)
            return carry

        lax.fori_loop(0, 16, body, 0)
        f, u = ("f", hp), ("u", hp)
        send(s1.at[hp, lo, yid[2], ra], fold.at[hp, 0], ydev[1], "f", f)
        send(s1.at[hp, hi, yid[2], ra], fold.at[hp, 1], ydev[3], "f", f)
        send(s1.at[hp, zid[2], lo, rb], fold.at[hp, 2], zdev[1], "f", f)
        send(s1.at[hp, zid[2], hi, rb], fold.at[hp, 3], zdev[3], "f", f)
        send(s1.at[hp, hi, yid[1], ra], recv2.at[hp, 0, hi], ydev[1], "u", u)
        send(s1.at[hp, lo, yid[3], ra], recv2.at[hp, 1, lo], ydev[3], "u", u)
        send(s1.at[hp, zid[1], hi, rb], recv2.at[hp, 2, hi], zdev[1], "u", u)
        send(s1.at[hp, zid[3], lo, rb], recv2.at[hp, 3, lo], zdev[3], "u", u)

    def rs_fold(hp):
        def add(k, index):
            for i in range(2):
                at = index(i)
                s1[at] = (s1[at].astype(F32) + fold[hp, k, i].astype(F32)).astype(BF)

        u = ("u", hp)
        arrived(("f", hp), fold.at[hp])
        add(0, lambda i: (hp, i, yid[1], ra))
        add(1, lambda i: (hp, 2 + i, yid[3], ra))
        add(2, lambda i: (hp, zid[1], i, rb))
        add(3, lambda i: (hp, zid[3], 2 + i, rb))
        send(s1.at[hp, lo, yid[1], ra], recv2.at[hp, 0, lo], ydev[1], "u", u)
        send(s1.at[hp, hi, yid[3], ra], recv2.at[hp, 1, hi], ydev[3], "u", u)
        send(s1.at[hp, zid[1], lo, rb], recv2.at[hp, 2, lo], zdev[1], "u", u)
        send(s1.at[hp, zid[3], hi, rb], recv2.at[hp, 3, hi], zdev[3], "u", u)

    def rs_second(hp):
        arrived(("u", hp), recv2.at[hp])
        for i in range(4):
            s2[hp, 0, i] = (
                s1[hp, i, y, ra].astype(F32)
                + recv2[hp, 0, i].astype(F32)
                + recv2[hp, 1, i].astype(F32)
            ).astype(BF)
            s2[hp, 1, i] = (
                s1[hp, z, i, rb].astype(F32)
                + recv2[hp, 2, i].astype(F32)
                + recv2[hp, 3, i].astype(F32)
            ).astype(BF)
        for r in (1, 3, 2):
            send(s2.at[hp, 0, zid[r]], recv3.at[hp, 0, r - 1], zdev[r], "t", ("t", hp))
            send(s2.at[hp, 1, yid[r]], recv3.at[hp, 1, r - 1], ydev[r], "t", ("t", hp))

    def rs_finish(hp):
        arrived(("t", hp), recv3.at[hp])
        cols = pl.ds(128 * hp, 128)
        for part, own in ((0, z), (1, y)):
            total = s2[hp, part, own].astype(F32)
            for r in range(3):
                total += recv3[hp, part, r].astype(F32)
            rows = pl.ds(48 * part, 48)
            for m in range(3):
                gw_ref[m, rows, cols] = total[:, 128 * m : 128 * m + 128]

    def dx_block(t, s):
        return dot(w[slot[s], :], g[256 * t : 256 * t + 256, :], NT)

    half_a, half_b = pl.ds(0, 384), pl.ds(384, 384)

    def dx_opposite(t):
        out = dx_block(t, 3).astype(BF)
        dx_send[t, 0] = out[:384]
        dx_send[t, 1] = out[384:]
        send(dx_send.at[t, 0], dx_fold.at[t, 0], right, "d", ("df", t))
        send(dx_send.at[t, 1], dx_fold.at[t, 1], left, "d", ("df", t))

    def dx_direct(t):
        out = dx_block(t, 2).astype(BF)
        dx_send[t, 2] = out[384:]
        send(dx_send.at[t, 2], dx_recv.at[t, 0, half_b], right, "d", ("d", t))
        dx_part[t, 0] = out[:384]
        out = dx_block(t, 1).astype(BF)
        dx_send[t, 3] = out[:384]
        send(dx_send.at[t, 3], dx_recv.at[t, 1, half_a], left, "d", ("d", t))
        dx_part[t, 1] = out[384:]

    def dx_folded(t):
        arrived(("df", t), dx_fold.at[t])
        dx_send[t, 4] = (dx_part[t, 0].astype(F32) + dx_fold[t, 0].astype(F32)).astype(BF)
        send(dx_send.at[t, 4], dx_recv.at[t, 0, half_a], right, "d", ("d", t))
        dx_send[t, 5] = (dx_part[t, 1].astype(F32) + dx_fold[t, 1].astype(F32)).astype(BF)
        send(dx_send.at[t, 5], dx_recv.at[t, 1, half_b], left, "d", ("d", t))

    def dx_mine(t):
        dx_own[t] = dx_block(t, 0).astype(BF)

    def dx_finish(t):
        arrived(("d", t), dx_recv.at[t])
        total = (
            dx_own[t].astype(F32) + dx_recv[t, 0].astype(F32) + dx_recv[t, 1].astype(F32)
        )
        gx_ref[pl.ds(256 * t, 256), :] = total.T.astype(BF)

    def bias_line():
        for hp in range(3):
            for par in range(2):
                total = jnp.zeros((8, 512), F32)
                for a in range(48):
                    part = gbias[hp, pl.ds(8 * a, 8), pl.ds(128 * par, 128)]
                    part = jnp.concatenate([part, jnp.zeros((8, 384), F32)], axis=1)
                    total += pltpu.roll(part, (512 - 8 * a) % 512, 1)
                sub = lax.broadcasted_iota(jnp.int32, (8, 512), 0)
                for bit in range(3):
                    moved = pltpu.roll(total, 512 - (1 << bit), 1)
                    total = jnp.where((sub >> bit) % 2 == 1, moved, total)
                h = 2 * hp + par
                gl[h : h + 1, :] = jnp.sum(total, axis=0, keepdims=True)
        gl[6:8, :] = jnp.zeros((2, 512), F32)

    attention()
    dx_opposite(0)
    dx_direct(0)
    transpose_rows(order[2])
    transpose_rows(order[3])
    finish_grads(0)
    weight_grad(0)
    finish_grads(1)
    weight_grad(1)
    dx_folded(0)
    rs_start(0)
    finish_grads(2)
    weight_grad(2)
    dx_opposite(1)
    rs_fold(0)
    rs_start(1)
    dx_direct(1)
    rs_start(2)
    rs_fold(1)
    dx_mine(0)
    bias_line()
    send(gl, gl_c, partner, "gc", "gc")
    rs_second(0)
    dx_mine(1)
    rs_fold(2)
    arrived("gc", gl_c)
    gl_s[0] = gl[...] + gl_c[...]
    for r in (1, 2, 3):
        send(gl_s.at[0], gl_r.at[r - 1], ydev[r], "gr", "gy")
    dx_folded(1)
    rs_second(1)
    arrived("gy", gl_r.at[pl.ds(0, 3)])
    gl_s[1] = gl_s[0] + gl_r[0] + gl_r[1] + gl_r[2]
    for r in (1, 2, 3):
        send(gl_s.at[1], gl_r.at[2 + r], zdev[r], "gr", "gz")
    rs_finish(0)
    dx_finish(0)
    rs_second(2)
    rs_finish(1)
    arrived("gz", gl_r.at[pl.ds(3, 3)])
    total = gl_s[1] + gl_r[3] + gl_r[4] + gl_r[5]
    far = jnp.sum(jnp.where(lane < 128, total, 0.0), axis=1, keepdims=True)
    total = jnp.where(lane == 0, far, total)
    total = pltpu.roll(total, 512 - 193, 1)
    gb_ref[...] = total[0:6, 0:320]
    rs_finish(2)
    dx_finish(1)
    sent("x", xbuf.at[:, pl.ds(0, 2304)])
    sent("h", kext.at[:, pl.ds(0, 512)])
    sent("hb", hb_send)
    sent("c", crecv)
    sent("f", fold)
    sent("u", recv2)
    sent("t", recv3)
    sent("d", dx_send)
    sent("gc", gl_c)
    sent("gr", gl_r)
    assert len(sends) == SENDS and len(recvs) == RECVS, (len(sends), len(recvs))


def write_out(gx, gw, gb, gx_out, gwq_out, gwk_out, gwv_out, gb_out, sem):
    pairs = [(gx, gx_out), (gw.at[0], gwq_out), (gw.at[1], gwk_out), (gw.at[2], gwv_out), (gb, gb_out)]
    copies = [pltpu.make_async_copy(a, b, sem.at[i]) for i, (a, b) in enumerate(pairs)]
    for cp in copies:
        cp.start()
    for cp in copies:
        cp.wait()


def local(inputs, w_query, w_key, w_value, rel_bias, d_out):
    any_spec = pl.BlockSpec(memory_space=pl.ANY)
    vmem = pl.BlockSpec(memory_space=pltpu.VMEM)
    V = pltpu.VMEM
    gx, gw, gb = pl.pallas_call(
        kernel,
        out_shape=(V((512, 768), BF), V((3, 96, 384), F32), V((6, 320), F32)),
        in_specs=[any_spec] * 6,
        out_specs=(vmem, vmem, vmem),
        scratch_shapes=[
            V((512, 3072), BF),
            V((3072, 1152), BF),
            V((4, 768, 512), BF),
            V((2, 3, 128, 384), F32),
            V((3, 768, 128), BF),
            V((3, 768, 128), BF),
            V((3, 512, 128), BF),
            V((512, 384), BF),
            V((3, 128, 768), BF),
            V((3, 768, 128), F32),
            V((3, 768, 128), F32),
            V((3, 384, 256), F32),
            V((3, 384, 256), F32),
            V((512, 1152), BF),
            V((3, 2, 256, 128), BF),
            V((3, 2, 256, 128), BF),
            V((3, 16, 2, 96, 384), BF),
            V((3, 16, 96, 384), BF),
            V((3, 4, 4, 96, 384), BF),
            V((3, 4, 2, 48, 384), BF),
            V((3, 4, 4, 48, 384), BF),
            V((3, 2, 4, 48, 384), BF),
            V((3, 2, 3, 48, 384), BF),
            V((2, 6, 384, 256), BF),
            V((2, 2, 384, 256), BF),
            V((2, 2, 768, 256), BF),
            V((2, 2, 384, 256), BF),
            V((2, 768, 256), BF),
            V((6, 320), F32),
            V((8, 512), F32),
            V((8, 512), F32),
            V((2, 8, 512), F32),
            V((6, 8, 512), F32),
            pltpu.SemaphoreType.DMA,
            pltpu.SemaphoreType.DMA,
            pltpu.SemaphoreType.DMA,
            pltpu.SemaphoreType.DMA,
            pltpu.SemaphoreType.DMA((SENDS,)),
            pltpu.SemaphoreType.DMA((RECVS,)),
        ],
        compiler_params=pltpu.CompilerParams(
            collective_id=0, has_side_effects=True, vmem_limit_bytes=58 * 1024 * 1024
        ),
    )(inputs, w_query, w_key, w_value, rel_bias.T, d_out)
    gx, gwq, gwk, gwv, gb = pl.pallas_call(
        write_out,
        out_shape=(
            jax.ShapeDtypeStruct((512, 768), BF),
            jax.ShapeDtypeStruct((96, 384), F32),
            jax.ShapeDtypeStruct((96, 384), F32),
            jax.ShapeDtypeStruct((96, 384), F32),
            jax.ShapeDtypeStruct((6, 320), F32),
        ),
        in_specs=[vmem] * 3,
        out_specs=[any_spec] * 5,
        scratch_shapes=[pltpu.SemaphoreType.DMA((5,))],
        compiler_params=pltpu.CompilerParams(vmem_limit_bytes=4 * 1024 * 1024),
    )(gx, gw, gb)
    return gx, gwq, gwk, gwv, gb.T


def solution(mesh):
    torus = Mesh(mesh.devices.reshape(4, 4, 2, mesh.shape["tp"]), ("sp_0", "sp_1", "sp_2", "tp"))
    return jax.shard_map(
        local,
        mesh=torus,
        in_specs=(
            P(SP, "tp"),
            P(None, "tp"),
            P(None, "tp"),
            P(None, "tp"),
            P(None, "tp"),
            P(SP, "tp"),
        ),
        out_specs=(P(SP, "tp"), P(SP, "tp"), P(SP, "tp"), P(SP, "tp"), P(None, "tp")),
        check_vma=False,
    )
```

time: 83.7 us -> 77.5 us (0.926)
  Pallas kernels: 82.7 us -> 76.6 us
    pallas_call x1, Pallas kernels: 81.7 us -> 75.5 us  [local(): pl.pallas_call(kernel, out_shape=(V((512, 768), BF), V((3, 96, 384), F32)...]
where the time goes in v1:
time: 77.5 us; the launch traced here: 77.4 us
  Pallas kernels  76.6 us (99%)
  between operations  0.8 us (1%)
    pallas_call x1, Pallas kernels, local(): pl.pallas_call(kernel, out_shape=(V((512, 768), BF), V((3, 96, 384), F32)...  75.5 us

profile of v1, /device:TPU:0, one launch (start us, length us, event | category | flops | bytes accessed | tf_op | source)
XLA Modules:
  0.0 77.4 jit_solution(17688172493661051324)
XLA Ops:
  0.6 75.5 %shard_map.101 = (bf16[512,768]{1,0:T(8,128)(2,1)S(1)}, f32[3,96,384]{2,1,0:T(8,128)S(1)}, f32[6,320]{1,0:T(8,128)S(1)}) custom-call(bf16[512,768]{1,0:T(8,128)(2,1)} %x_hbm.1, bf16[3072,384]{1,0:T(8,128)(2,1)} %wq_hbm.1, bf16[3072,384]{1,0:T(8,128)(2,1)} %wk_hbm.1, bf16[3072,384]{1,0:T(8,128)(2,1)} %wv_hbm.1, f32[6,320]{1,0:T(8,128)} %bitcast.2, ...), custom_call_target="tpu_custom_call" | custom-call | tf_op jit(solution)/shard_map/pallas_call | solution.py:455
  76.2 1.1 %shard_map.102 = (bf16[512,768]{1,0:T(8,128)(2,1)}, f32[96,384]{1,0:T(8,128)}, f32[96,384]{1,0:T(8,128)}, f32[96,384]{1,0:T(8,128)}, f32[6,320]{1,0:T(8,128)}) custom-call(bf16[512,768]{1,0:T(8,128)(2,1)S(1)} %get-tuple-element.13.gx, f32[3,96,384]{2,1,0:T(8,128)S(1)} %get-tuple-element.14.gw, f32[6,320]{1,0:T(8,128)S(1)} %get-tuple-element.15.gb), custom_call_target="tpu_custom_call" | custom-call | tf_op jit(solution)/shard_map/pallas_call | solution.py:505

commit v2 on v1

--- a/solution.py
+++ b/solution.py
@@ -120,9 +120,9 @@
                 else:
                     vext[hp, ext] = one
 
-    def transpose_rows(j):
+    def transpose_rows(j, slots=(0, 1, 2, 3)):
         rows = pl.ds(128 * j, 128)
-        for s in range(4):
+        for s in slots:
             xt[src[s], :, rows] = xbuf[rows, slot[s]].T
 
     send_own(order[0])
@@ -170,6 +170,7 @@
     send(kext.at[:, pl.ds(512, 256)], kext.at[:, pl.ds(0, 256)], sp_next, "h", "hk")
     send(vext.at[:, pl.ds(512, 256)], vext.at[:, pl.ds(0, 256)], sp_next, "h", "hv")
     transpose_rows(order[1])
+    transpose_rows(order[2], (0, 1, 2))
     forward(order[3])
     project_a(order[3])
     project_b(order[2])
@@ -221,20 +222,26 @@
     for hp in range(3):
         kt[hp, :, 0:256] = kext[hp, 0:256].T
 
-    def attention():
-        for hp in range(3):
+    def send_halo_grads(heads):
+        for hp in heads:
+            hb_send[hp, 0] = dk_acc[hp, 0:256].astype(BF)
+            hb_send[hp, 1] = dv_acc[hp, 0:256].astype(BF)
+        for hp in heads:
+            send(hb_send.at[hp], hb_recv.at[hp], sp_prev, "hb", ("hb", hp))
+
+    def attention_first():
+        for hp in (0, 1):
             unit(hp, 0)
             unit(hp, 1)
-        for hp in range(3):
-            hb_send[hp, 0] = dk_acc[hp, 0:256].astype(BF)
-            hb_send[hp, 1] = dv_acc[hp, 0:256].astype(BF)
-        for hp in range(3):
-            send(hb_send.at[hp], hb_recv.at[hp], sp_prev, "hb", ("hb", hp))
-        for hp in range(3):
-            unit(hp, 2)
+        send_halo_grads((0, 1))
+
+    def attention_rest():
+        for hp, qp in ((2, 0), (2, 1), (0, 2), (1, 2), (2, 2)):
+            unit(hp, qp)
         for hp in range(3):
             g[0:256, pl.ds(384 + 128 * hp, 128)] = dk_acc[hp, 256:512].astype(BF)
             g[0:256, pl.ds(768 + 128 * hp, 128)] = dv_acc[hp, 256:512].astype(BF)
+        send_halo_grads((2,))
 
     def finish_grads(hp):
         arrived(("hb", hp), hb_recv.at[hp])
@@ -245,116 +252,110 @@
             dv_acc[hp, 512:768] + hb_recv[hp, 1].astype(F32)
         ).astype(BF)
 
-    def weight_grad(hp):
-        def body(i, carry):
-            grads = jnp.concatenate(
-                [g[:, 384 * m + 128 * hp : 384 * m + 128 * hp + 128] for m in range(3)], axis=1
-            )
-            out = dot(xt[i], grads).astype(BF)
-            dwb[hp, pl.ds(4 * i, 4)] = out.reshape(4, 2, 96, 384)
-            return carry
-
-        lax.fori_loop(0, 4, body, 0)
-        send(dwb.at[hp, :, 1 - c], crecv.at[hp], partner, "c", ("c", hp))
+    def weight_grad(m):
+        for i in range(4):
+            out = dot(xt[i], g[:, 384 * m : 384 * m + 384]).astype(BF)
+            part = pl.ds(4 * i, 4)
+            dwb[m, part] = out.reshape(4, 2, 96, 384)
+            send(dwb.at[m, part, 1 - c], crecv.at[m, part], partner, "c", ("c", m))
 
     lo, hi = pl.ds(0, 2), pl.ds(2, 2)
     ra, rb = pl.ds(0, 48), pl.ds(48, 48)
 
-    def rs_start(hp):
-        arrived(("c", hp), crecv.at[hp])
+    def rs_start(m):
+        arrived(("c", m), crecv.at[m])
 
         def body(i, carry):
             zz, yy = i // 4, i % 4
-            s1[hp, zz, yy] = (dwb[hp, i, c].astype(F32) + crecv[hp, i].astype(F32)).astype(BF)
+            s1[m, zz, yy] = (dwb[m, i, c].astype(F32) + crecv[m, i].astype(F32)).astype(BF)
             return carry
 
         lax.fori_loop(0, 16, body, 0)
-        f, u = ("f", hp), ("u", hp)
-        send(s1.at[hp, lo, yid[2], ra], fold.at[hp, 0], ydev[1], "f", f)
-        send(s1.at[hp, hi, yid[2], ra], fold.at[hp, 1], ydev[3], "f", f)
-        send(s1.at[hp, zid[2], lo, rb], fold.at[hp, 2], zdev[1], "f", f)
-        send(s1.at[hp, zid[2], hi, rb], fold.at[hp, 3], zdev[3], "f", f)
-        send(s1.at[hp, hi, yid[1], ra], recv2.at[hp, 0, hi], ydev[1], "u", u)
-        send(s1.at[hp, lo, yid[3], ra], recv2.at[hp, 1, lo], ydev[3], "u", u)
-        send(s1.at[hp, zid[1], hi, rb], recv2.at[hp, 2, hi], zdev[1], "u", u)
-        send(s1.at[hp, zid[3], lo, rb], recv2.at[hp, 3, lo], zdev[3], "u", u)
-
-    def rs_fold(hp):
+        f, u = ("f", m), ("u", m)
+        send(s1.at[m, lo, yid[2], ra], fold.at[m, 0], ydev[1], "f", f)
+        send(s1.at[m, hi, yid[2], ra], fold.at[m, 1], ydev[3], "f", f)
+        send(s1.at[m, zid[2], lo, rb], fold.at[m, 2], zdev[1], "f", f)
+        send(s1.at[m, zid[2], hi, rb], fold.at[m, 3], zdev[3], "f", f)
+        send(s1.at[m, hi, yid[1], ra], recv2.at[m, 0, hi], ydev[1], "u", u)
+        send(s1.at[m, lo, yid[3], ra], recv2.at[m, 1, lo], ydev[3], "u", u)
+        send(s1.at[m, zid[1], hi, rb], recv2.at[m, 2, hi], zdev[1], "u", u)
+        send(s1.at[m, zid[3], lo, rb], recv2.at[m, 3, lo], zdev[3], "u", u)
+
+    def rs_fold(m):
         def add(k, index):
             for i in range(2):
                 at = index(i)
-                s1[at] = (s1[at].astype(F32) + fold[hp, k, i].astype(F32)).astype(BF)
-
-        u = ("u", hp)
-        arrived(("f", hp), fold.at[hp])
-        add(0, lambda i: (hp, i, yid[1], ra))
-        add(1, lambda i: (hp, 2 + i, yid[3], ra))
-        add(2, lambda i: (hp, zid[1], i, rb))
-        add(3, lambda i: (hp, zid[3], 2 + i, rb))
-        send(s1.at[hp, lo, yid[1], ra], recv2.at[hp, 0, lo], ydev[1], "u", u)
-        send(s1.at[hp, hi, yid[3], ra], recv2.at[hp, 1, hi], ydev[3], "u", u)
-        send(s1.at[hp, zid[1], lo, rb], recv2.at[hp, 2, lo], zdev[1], "u", u)
-        send(s1.at[hp, zid[3], hi, rb], recv2.at[hp, 3, hi], zdev[3], "u", u)
-
-    def rs_second(hp):
-        arrived(("u", hp), recv2.at[hp])
+                s1[at] = (s1[at].astype(F32) + fold[m, k, i].astype(F32)).astype(BF)
+
+        u = ("u", m)
+        arrived(("f", m), fold.at[m])
+        add(0, lambda i: (m, i, yid[1], ra))
+        add(1, lambda i: (m, 2 + i, yid[3], ra))
+        add(2, lambda i: (m, zid[1], i, rb))
+        add(3, lambda i: (m, zid[3], 2 + i, rb))
+        send(s1.at[m, lo, yid[1], ra], recv2.at[m, 0, lo], ydev[1], "u", u)
+        send(s1.at[m, hi, yid[3], ra], recv2.at[m, 1, hi], ydev[3], "u", u)
+        send(s1.at[m, zid[1], lo, rb], recv2.at[m, 2, lo], zdev[1], "u", u)
+        send(s1.at[m, zid[3], hi, rb], recv2.at[m, 3, hi], zdev[3], "u", u)
+
+    def rs_second(m):
+        arrived(("u", m), recv2.at[m])
         for i in range(4):
-            s2[hp, 0, i] = (
-                s1[hp, i, y, ra].astype(F32)
-                + recv2[hp, 0, i].astype(F32)
-                + recv2[hp, 1, i].astype(F32)
+            s2[m, 0, i] = (
+                s1[m, i, y, ra].astype(F32)
+                + recv2[m, 0, i].astype(F32)
+                + recv2[m, 1, i].astype(F32)
             ).astype(BF)
-            s2[hp, 1, i] = (
-                s1[hp, z, i, rb].astype(F32)
-                + recv2[hp, 2, i].astype(F32)
-                + recv2[hp, 3, i].astype(F32)
+            s2[m, 1, i] = (
+                s1[m, z, i, rb].astype(F32)
+                + recv2[m, 2, i].astype(F32)
+                + recv2[m, 3, i].astype(F32)
             ).astype(BF)
         for r in (1, 3, 2):
-            send(s2.at[hp, 0, zid[r]], recv3.at[hp, 0, r - 1], zdev[r], "t", ("t", hp))
-            send(s2.at[hp, 1, yid[r]], recv3.at[hp, 1, r - 1], ydev[r], "t", ("t", hp))
-
-    def rs_finish(hp):
-        arrived(("t", hp), recv3.at[hp])
-        cols = pl.ds(128 * hp, 128)
+            send(s2.at[m, 0, zid[r]], recv3.at[m, 0, r - 1], zdev[r], "t", ("t", m))
+            send(s2.at[m, 1, yid[r]], recv3.at[m, 1, r - 1], ydev[r], "t", ("t", m))
+
+    def rs_finish(m):
+        arrived(("t", m), recv3.at[m])
         for part, own in ((0, z), (1, y)):
-            total = s2[hp, part, own].astype(F32)
+            total = s2[m, part, own].astype(F32)
             for r in range(3):
-                total += recv3[hp, part, r].astype(F32)
-            rows = pl.ds(48 * part, 48)
-            for m in range(3):
-                gw_ref[m, rows, cols] = total[:, 128 * m : 128 * m + 128]
-
-    def dx_block(t, s):
-        return dot(w[slot[s], :], g[256 * t : 256 * t + 256, :], NT)
+                total += recv3[m, part, r].astype(F32)
+            gw_ref[m, pl.ds(48 * part, 48), :] = total
+
+    def dx_block(t, s, start=0, size=768):
+        rows = slice(768 * s + start, 768 * s + start + size)
+        return dot(w[rows, :], g[256 * t : 256 * t + 256, :], NT).astype(BF)
 
     half_a, half_b = pl.ds(0, 384), pl.ds(384, 384)
 
     def dx_opposite(t):
-        out = dx_block(t, 3).astype(BF)
-        dx_send[t, 0] = out[:384]
-        dx_send[t, 1] = out[384:]
+        first, second = dx_block(t, 3, 0, 384), dx_block(t, 3, 384, 384)
+        dx_send[t, 0] = first
+        dx_send[t, 1] = second
         send(dx_send.at[t, 0], dx_fold.at[t, 0], right, "d", ("df", t))
         send(dx_send.at[t, 1], dx_fold.at[t, 1], left, "d", ("df", t))
 
     def dx_direct(t):
-        out = dx_block(t, 2).astype(BF)
-        dx_send[t, 2] = out[384:]
+        for_right, for_left = dx_block(t, 2), dx_block(t, 1)
+        dx_send[t, 2] = for_right[384:]
+        dx_part[t, 0] = for_right[:384]
+        dx_send[t, 3] = for_left[:384]
+        dx_part[t, 1] = for_left[384:]
         send(dx_send.at[t, 2], dx_recv.at[t, 0, half_b], right, "d", ("d", t))
-        dx_part[t, 0] = out[:384]
-        out = dx_block(t, 1).astype(BF)
-        dx_send[t, 3] = out[:384]
         send(dx_send.at[t, 3], dx_recv.at[t, 1, half_a], left, "d", ("d", t))
-        dx_part[t, 1] = out[384:]
 
     def dx_folded(t):
         arrived(("df", t), dx_fold.at[t])
         dx_send[t, 4] = (dx_part[t, 0].astype(F32) + dx_fold[t, 0].astype(F32)).astype(BF)
+        dx_send[t, 5] = (dx_part[t, 1].astype(F32) + dx_fold[t, 1].astype(F32)).astype(BF)
         send(dx_send.at[t, 4], dx_recv.at[t, 0, half_a], right, "d", ("d", t))
-        dx_send[t, 5] = (dx_part[t, 1].astype(F32) + dx_fold[t, 1].astype(F32)).astype(BF)
         send(dx_send.at[t, 5], dx_recv.at[t, 1, half_b], left, "d", ("d", t))
 
-    def dx_mine(t):
-        dx_own[t] = dx_block(t, 0).astype(BF)
+    def dx_mine():
+        first, second = dx_block(0, 0), dx_block(1, 0)
+        dx_own[0] = first
+        dx_own[1] = second
 
     def dx_finish(t):
         arrived(("d", t), dx_recv.at[t])
@@ -379,45 +380,46 @@
                 gl[h : h + 1, :] = jnp.sum(total, axis=0, keepdims=True)
         gl[6:8, :] = jnp.zeros((2, 512), F32)
 
-    attention()
+    attention_first()
+    attention_rest()
     dx_opposite(0)
     dx_direct(0)
-    transpose_rows(order[2])
+    transpose_rows(order[2], (3,))
     transpose_rows(order[3])
-    finish_grads(0)
     weight_grad(0)
-    finish_grads(1)
-    weight_grad(1)
-    dx_folded(0)
-    rs_start(0)
-    finish_grads(2)
-    weight_grad(2)
-    dx_opposite(1)
-    rs_fold(0)
-    rs_start(1)
-    dx_direct(1)
-    rs_start(2)
-    rs_fold(1)
-    dx_mine(0)
     bias_line()
     send(gl, gl_c, partner, "gc", "gc")
-    rs_second(0)
-    dx_mine(1)
-    rs_fold(2)
+    finish_grads(0)
+    finish_grads(1)
+    finish_grads(2)
+    dx_opposite(1)
     arrived("gc", gl_c)
     gl_s[0] = gl[...] + gl_c[...]
     for r in (1, 2, 3):
         send(gl_s.at[0], gl_r.at[r - 1], ydev[r], "gr", "gy")
-    dx_folded(1)
-    rs_second(1)
+    rs_start(0)
+    weight_grad(1)
+    dx_folded(0)
+    dx_direct(1)
     arrived("gy", gl_r.at[pl.ds(0, 3)])
     gl_s[1] = gl_s[0] + gl_r[0] + gl_r[1] + gl_r[2]
     for r in (1, 2, 3):
         send(gl_s.at[1], gl_r.at[2 + r], zdev[r], "gr", "gz")
+    rs_start(1)
+    rs_fold(0)
+    weight_grad(2)
+    rs_start(2)
+    rs_fold(1)
+    dx_mine()
+    dx_folded(1)
+    rs_second(0)
+    rs_fold(2)
+    rs_second(1)
+    dx_finish(0)
     rs_finish(0)
-    dx_finish(0)
     rs_second(2)
     rs_finish(1)
+    dx_finish(1)
     arrived("gz", gl_r.at[pl.ds(3, 3)])
     total = gl_s[1] + gl_r[3] + gl_r[4] + gl_r[5]
     far = jnp.sum(jnp.where(lane < 128, total, 0.0), axis=1, keepdims=True)
@@ -425,7 +427,6 @@
     total = pltpu.roll(total, 512 - 193, 1)
     gb_ref[...] = total[0:6, 0:320]
     rs_finish(2)
-    dx_finish(1)
     sent("x", xbuf.at[:, pl.ds(0, 2304)])
     sent("h", kext.at[:, pl.ds(0, 512)])
     sent("hb", hb_send)

time: 77.5 us -> 74 us (0.955)
  Pallas kernels: 76.6 us -> 73 us
    pallas_call x1, Pallas kernels: 75.5 us -> 71.9 us  [local(): pl.pallas_call(kernel, out_shape=(V((512, 768), BF), V((3, 96, 384), F32)...]
where the time goes in v2:
time: 74 us; the launch traced here: 73.8 us
  Pallas kernels  73 us (99%)
  between operations  0.82 us (1%)
    pallas_call x1, Pallas kernels, local(): pl.pallas_call(kernel, out_shape=(V((512, 768), BF), V((3, 96, 384), F32)...  71.9 us

profile of v2, /device:TPU:0, one launch (start us, length us, event | category | flops | bytes accessed | tf_op | source)
XLA Modules:
  0.0 73.8 jit_solution(14292280217681090519)
XLA Ops:
  0.6 71.9 %shard_map.101 = (bf16[512,768]{1,0:T(8,128)(2,1)S(1)}, f32[3,96,384]{2,1,0:T(8,128)S(1)}, f32[6,320]{1,0:T(8,128)S(1)}) custom-call(bf16[512,768]{1,0:T(8,128)(2,1)} %x_hbm.1, bf16[3072,384]{1,0:T(8,128)(2,1)} %wq_hbm.1, bf16[3072,384]{1,0:T(8,128)(2,1)} %wk_hbm.1, bf16[3072,384]{1,0:T(8,128)(2,1)} %wv_hbm.1, f32[6,320]{1,0:T(8,128)} %bitcast.2, ...), custom_call_target="tpu_custom_call" | custom-call | tf_op jit(solution)/shard_map/pallas_call | solution.py:456
  72.6 1.1 %shard_map.102 = (bf16[512,768]{1,0:T(8,128)(2,1)}, f32[96,384]{1,0:T(8,128)}, f32[96,384]{1,0:T(8,128)}, f32[96,384]{1,0:T(8,128)}, f32[6,320]{1,0:T(8,128)}) custom-call(bf16[512,768]{1,0:T(8,128)(2,1)S(1)} %get-tuple-element.13.gx, f32[3,96,384]{2,1,0:T(8,128)S(1)} %get-tuple-element.14.gw, f32[6,320]{1,0:T(8,128)S(1)} %get-tuple-element.15.gb), custom_call_target="tpu_custom_call" | custom-call | tf_op jit(solution)/shard_map/pallas_call | solution.py:506

commit v3 on v2

--- a/solution.py
+++ b/solution.py
@@ -12,7 +12,9 @@
 MESH = pl.DeviceIdType.MESH
 BF = jnp.bfloat16
 F32 = jnp.float32
-SENDS, RECVS = 10, 36
+SENDS, RECVS = 18, 36
+LO = 2
+CUTS = (0, 384, 896, 1152)
 
 NN = (((1,), (0,)), ((), ()))
 NT = (((1,), (1,)), ((), ()))
@@ -26,8 +28,7 @@
     x_hbm, wq_hbm, wk_hbm, wv_hbm, rb_hbm, do_hbm,
     gx_ref, gw_ref, gb_ref,
     xbuf, w, xt, acc, kext, vext, qs, do, kt, dk_acc, dv_acc, bias, gbias, g,
-    hb_send, hb_recv, dwb, crecv, s1,
-    fold, recv2, s2, recv3,
+    hb_send, hb_recv, dwbs, crecvs, s1s, folds, recv2s, s2s, recv3s,
     dx_send, dx_fold, dx_recv, dx_part, dx_own,
     rbuf, gl, gl_c, gl_s, gl_r,
     lsem_x, lsem_b, lsem_w, lsem_do, ssem, rsem,
@@ -253,75 +254,75 @@
         ).astype(BF)
 
     def weight_grad(m):
-        for i in range(4):
-            out = dot(xt[i], g[:, 384 * m : 384 * m + 384]).astype(BF)
-            part = pl.ds(4 * i, 4)
-            dwb[m, part] = out.reshape(4, 2, 96, 384)
-            send(dwb.at[m, part, 1 - c], crecv.at[m, part], partner, "c", ("c", m))
-
-    lo, hi = pl.ds(0, 2), pl.ds(2, 2)
+        dwb, crecv = dwbs[m], crecvs[m]
+        width = CUTS[m + 1] - CUTS[m]
+        step = 1 if width > 256 else 2
+        for first in range(0, 4, step):
+            blocks = range(first, first + step)
+            outs = [dot(xt[i], g[:, CUTS[m] : CUTS[m + 1]]).astype(BF) for i in blocks]
+            for i, out in zip(blocks, outs):
+                dwb[4 * i : 4 * i + 4] = out.reshape(4, 2, 96, width)
+            part = pl.ds(4 * first, 4 * step)
+            send(dwb.at[part, 1 - c], crecv.at[part], partner, ("c", m), ("c", m))
+
+    lo, hi = pl.ds(0, LO), pl.ds(LO, 4 - LO)
     ra, rb = pl.ds(0, 48), pl.ds(48, 48)
 
     def rs_start(m):
-        arrived(("c", m), crecv.at[m])
+        dwb, crecv, s1, fold, recv2 = dwbs[m], crecvs[m], s1s[m], folds[m], recv2s[m]
+        arrived(("c", m), crecv)
 
         def body(i, carry):
             zz, yy = i // 4, i % 4
-            s1[m, zz, yy] = (dwb[m, i, c].astype(F32) + crecv[m, i].astype(F32)).astype(BF)
+            s1[zz, yy] = (dwb[i, c].astype(F32) + crecv[i].astype(F32)).astype(BF)
             return carry
 
         lax.fori_loop(0, 16, body, 0)
         f, u = ("f", m), ("u", m)
-        send(s1.at[m, lo, yid[2], ra], fold.at[m, 0], ydev[1], "f", f)
-        send(s1.at[m, hi, yid[2], ra], fold.at[m, 1], ydev[3], "f", f)
-        send(s1.at[m, zid[2], lo, rb], fold.at[m, 2], zdev[1], "f", f)
-        send(s1.at[m, zid[2], hi, rb], fold.at[m, 3], zdev[3], "f", f)
-        send(s1.at[m, hi, yid[1], ra], recv2.at[m, 0, hi], ydev[1], "u", u)
-        send(s1.at[m, lo, yid[3], ra], recv2.at[m, 1, lo], ydev[3], "u", u)
-        send(s1.at[m, zid[1], hi, rb], recv2.at[m, 2, hi], zdev[1], "u", u)
-        send(s1.at[m, zid[3], lo, rb], recv2.at[m, 3, lo], zdev[3], "u", u)
+        send(s1.at[lo, yid[2], ra], fold.at[0, lo], ydev[1], f, f)
+        send(s1.at[hi, yid[2], ra], fold.at[0, hi], ydev[3], f, f)
+        send(s1.at[zid[2], lo, rb], fold.at[1, lo], zdev[1], f, f)
+        send(s1.at[zid[2], hi, rb], fold.at[1, hi], zdev[3], f, f)
+        send(s1.at[hi, yid[1], ra], recv2.at[0, hi], ydev[1], u, u)
+        send(s1.at[lo, yid[3], ra], recv2.at[1, lo], ydev[3], u, u)
+        send(s1.at[zid[1], hi, rb], recv2.at[2, hi], zdev[1], u, u)
+        send(s1.at[zid[3], lo, rb], recv2.at[3, lo], zdev[3], u, u)
 
     def rs_fold(m):
-        def add(k, index):
-            for i in range(2):
-                at = index(i)
-                s1[at] = (s1[at].astype(F32) + fold[m, k, i].astype(F32)).astype(BF)
-
+        s1, fold, recv2 = s1s[m], folds[m], recv2s[m]
         u = ("u", m)
-        arrived(("f", m), fold.at[m])
-        add(0, lambda i: (m, i, yid[1], ra))
-        add(1, lambda i: (m, 2 + i, yid[3], ra))
-        add(2, lambda i: (m, zid[1], i, rb))
-        add(3, lambda i: (m, zid[3], 2 + i, rb))
-        send(s1.at[m, lo, yid[1], ra], recv2.at[m, 0, lo], ydev[1], "u", u)
-        send(s1.at[m, hi, yid[3], ra], recv2.at[m, 1, hi], ydev[3], "u", u)
-        send(s1.at[m, zid[1], lo, rb], recv2.at[m, 2, lo], zdev[1], "u", u)
-        send(s1.at[m, zid[3], hi, rb], recv2.at[m, 3, hi], zdev[3], "u", u)
+        arrived(("f", m), fold)
+        for i in range(4):
+            r = 1 if i < LO else 3
+            for part, at in enumerate(((i, yid[r], ra), (zid[r], i, rb))):
+                s1[at] = (s1[at].astype(F32) + fold[part, i].astype(F32)).astype(BF)
+        send(s1.at[lo, yid[1], ra], recv2.at[0, lo], ydev[1], u, u)
+        send(s1.at[hi, yid[3], ra], recv2.at[1, hi], ydev[3], u, u)
+        send(s1.at[zid[1], lo, rb], recv2.at[2, lo], zdev[1], u, u)
+        send(s1.at[zid[3], hi, rb], recv2.at[3, hi], zdev[3], u, u)
 
     def rs_second(m):
-        arrived(("u", m), recv2.at[m])
+        s1, recv2, s2, recv3 = s1s[m], recv2s[m], s2s[m], recv3s[m]
+        arrived(("u", m), recv2)
         for i in range(4):
-            s2[m, 0, i] = (
-                s1[m, i, y, ra].astype(F32)
-                + recv2[m, 0, i].astype(F32)
-                + recv2[m, 1, i].astype(F32)
+            s2[0, i] = (
+                s1[i, y, ra].astype(F32) + recv2[0, i].astype(F32) + recv2[1, i].astype(F32)
             ).astype(BF)
-            s2[m, 1, i] = (
-                s1[m, z, i, rb].astype(F32)
-                + recv2[m, 2, i].astype(F32)
-                + recv2[m, 3, i].astype(F32)
+            s2[1, i] = (
+                s1[z, i, rb].astype(F32) + recv2[2, i].astype(F32) + recv2[3, i].astype(F32)
             ).astype(BF)
         for r in (1, 3, 2):
-            send(s2.at[m, 0, zid[r]], recv3.at[m, 0, r - 1], zdev[r], "t", ("t", m))
-            send(s2.at[m, 1, yid[r]], recv3.at[m, 1, r - 1], ydev[r], "t", ("t", m))
+            send(s2.at[0, zid[r]], recv3.at[0, r - 1], zdev[r], ("t", m), ("t", m))
+            send(s2.at[1, yid[r]], recv3.at[1, r - 1], ydev[r], ("t", m), ("t", m))
 
     def rs_finish(m):
-        arrived(("t", m), recv3.at[m])
+        s2, recv3 = s2s[m], recv3s[m]
+        arrived(("t", m), recv3)
         for part, own in ((0, z), (1, y)):
-            total = s2[m, part, own].astype(F32)
+            total = s2[part, own].astype(F32)
             for r in range(3):
-                total += recv3[m, part, r].astype(F32)
-            gw_ref[m, pl.ds(48 * part, 48), :] = total
+                total += recv3[part, r].astype(F32)
+            gw_ref[pl.ds(48 * part, 48), CUTS[m] : CUTS[m + 1]] = total
 
     def dx_block(t, s, start=0, size=768):
         rows = slice(768 * s + start, 768 * s + start + size)
@@ -383,43 +384,43 @@
     attention_first()
     attention_rest()
     dx_opposite(0)
-    dx_direct(0)
     transpose_rows(order[2], (3,))
     transpose_rows(order[3])
     weight_grad(0)
-    bias_line()
-    send(gl, gl_c, partner, "gc", "gc")
+    dx_direct(0)
+    rs_start(0)
     finish_grads(0)
     finish_grads(1)
     finish_grads(2)
+    weight_grad(1)
     dx_opposite(1)
+    dx_folded(0)
+    rs_fold(0)
+    rs_start(1)
+    weight_grad(2)
+    dx_direct(1)
+    rs_start(2)
+    bias_line()
+    send(gl, gl_c, partner, "gc", "gc")
+    rs_second(0)
+    rs_fold(1)
     arrived("gc", gl_c)
     gl_s[0] = gl[...] + gl_c[...]
     for r in (1, 2, 3):
         send(gl_s.at[0], gl_r.at[r - 1], ydev[r], "gr", "gy")
-    rs_start(0)
-    weight_grad(1)
-    dx_folded(0)
-    dx_direct(1)
+    dx_folded(1)
+    dx_mine()
+    rs_fold(2)
+    dx_finish(0)
+    rs_second(1)
+    rs_second(2)
     arrived("gy", gl_r.at[pl.ds(0, 3)])
     gl_s[1] = gl_s[0] + gl_r[0] + gl_r[1] + gl_r[2]
     for r in (1, 2, 3):
         send(gl_s.at[1], gl_r.at[2 + r], zdev[r], "gr", "gz")
-    rs_start(1)
-    rs_fold(0)
-    weight_grad(2)
-    rs_start(2)
-    rs_fold(1)
-    dx_mine()
-    dx_folded(1)
-    rs_second(0)
-    rs_fold(2)
-    rs_second(1)
-    dx_finish(0)
     rs_finish(0)
-    rs_second(2)
+    dx_finish(1)
     rs_finish(1)
-    dx_finish(1)
     arrived("gz", gl_r.at[pl.ds(3, 3)])
     total = gl_s[1] + gl_r[3] + gl_r[4] + gl_r[5]
     far = jnp.sum(jnp.where(lane < 128, total, 0.0), axis=1, keepdims=True)
@@ -430,10 +431,11 @@
     sent("x", xbuf.at[:, pl.ds(0, 2304)])
     sent("h", kext.at[:, pl.ds(0, 512)])
     sent("hb", hb_send)
-    sent("c", crecv)
-    sent("f", fold)
-    sent("u", recv2)
-    sent("t", recv3)
+    for m in range(3):
+        sent(("c", m), crecvs[m])
+        sent(("f", m), folds[m])
+        sent(("u", m), recv2s[m])
+        sent(("t", m), recv3s[m])
     sent("d", dx_send)
     sent("gc", gl_c)
     sent("gr", gl_r)
@@ -441,7 +443,8 @@
 
 
 def write_out(gx, gw, gb, gx_out, gwq_out, gwk_out, gwv_out, gb_out, sem):
-    pairs = [(gx, gx_out), (gw.at[0], gwq_out), (gw.at[1], gwk_out), (gw.at[2], gwv_out), (gb, gb_out)]
+    gws = [gw.at[:, pl.ds(384 * m, 384)] for m in range(3)]
+    pairs = [(gx, gx_out), (gws[0], gwq_out), (gws[1], gwk_out), (gws[2], gwv_out), (gb, gb_out)]
     copies = [pltpu.make_async_copy(a, b, sem.at[i]) for i, (a, b) in enumerate(pairs)]
     for cp in copies:
         cp.start()
@@ -453,9 +456,13 @@
     any_spec = pl.BlockSpec(memory_space=pl.ANY)
     vmem = pl.BlockSpec(memory_space=pltpu.VMEM)
     V = pltpu.VMEM
+
+    def per_cut(*dims):
+        return tuple(V((*dims, b - a), BF) for a, b in zip(CUTS, CUTS[1:]))
+
     gx, gw, gb = pl.pallas_call(
         kernel,
-        out_shape=(V((512, 768), BF), V((3, 96, 384), F32), V((6, 320), F32)),
+        out_shape=(V((512, 768), BF), V((96, 1152), F32), V((6, 320), F32)),
         in_specs=[any_spec] * 6,
         out_specs=(vmem, vmem, vmem),
         scratch_shapes=[
@@ -475,13 +482,13 @@
             V((512, 1152), BF),
             V((3, 2, 256, 128), BF),
             V((3, 2, 256, 128), BF),
-            V((3, 16, 2, 96, 384), BF),
-            V((3, 16, 96, 384), BF),
-            V((3, 4, 4, 96, 384), BF),
-            V((3, 4, 2, 48, 384), BF),
-            V((3, 4, 4, 48, 384), BF),
-            V((3, 2, 4, 48, 384), BF),
-            V((3, 2, 3, 48, 384), BF),
+            per_cut(16, 2, 96),
+            per_cut(16, 96),
+            per_cut(4, 4, 96),
+            per_cut(2, 4, 48),
+            per_cut(4, 4, 48),
+            per_cut(2, 4, 48),
+            per_cut(2, 3, 48),
             V((2, 6, 384, 256), BF),
             V((2, 2, 384, 256), BF),
             V((2, 2, 768, 256), BF),

time: 74 us -> 73 us (0.986)
  Pallas kernels: 73 us -> 72.1 us
    pallas_call x1, Pallas kernels: 71.9 us -> 71 us  [local(): pl.pallas_call(kernel, out_shape=(V((512, 768), BF), V((96, 1152), F32),...]
where the time goes in v3:
time: 73 us; the launch traced here: 72.9 us
  Pallas kernels  72.1 us (99%)
  between operations  0.82 us (1%)
    pallas_call x1, Pallas kernels, local(): pl.pallas_call(kernel, out_shape=(V((512, 768), BF), V((96, 1152), F32),...  71 us

profile of v3, /device:TPU:0, one launch (start us, length us, event | category | flops | bytes accessed | tf_op | source)
XLA Modules:
  0.0 72.9 jit_solution(11351295439219954019)
XLA Ops:
  0.6 71.0 %shard_map.101 = (bf16[512,768]{1,0:T(8,128)(2,1)S(1)}, f32[96,1152]{1,0:T(8,128)S(1)}, f32[6,320]{1,0:T(8,128)S(1)}) custom-call(bf16[512,768]{1,0:T(8,128)(2,1)} %x_hbm.1, bf16[3072,384]{1,0:T(8,128)(2,1)} %wq_hbm.1, bf16[3072,384]{1,0:T(8,128)(2,1)} %wk_hbm.1, bf16[3072,384]{1,0:T(8,128)(2,1)} %wv_hbm.1, f32[6,320]{1,0:T(8,128)} %bitcast.2, ...), custom_call_target="tpu_custom_call" | custom-call | tf_op jit(solution)/shard_map/pallas_call | solution.py:463
  71.7 1.1 %shard_map.102 = (bf16[512,768]{1,0:T(8,128)(2,1)}, f32[96,384]{1,0:T(8,128)}, f32[96,384]{1,0:T(8,128)}, f32[96,384]{1,0:T(8,128)}, f32[6,320]{1,0:T(8,128)}) custom-call(bf16[512,768]{1,0:T(8,128)(2,1)S(1)} %get-tuple-element.13.gx, f32[96,1152]{1,0:T(8,128)S(1)} %get-tuple-element.14.gw, f32[6,320]{1,0:T(8,128)S(1)} %get-tuple-element.15.gb), custom_call_target="tpu_custom_call" | custom-call | tf_op jit(solution)/shard_map/pallas_call | solution.py:513

commit v4 on v3

--- a/solution.py
+++ b/solution.py
@@ -274,10 +274,10 @@
 
         def body(i, carry):
             zz, yy = i // 4, i % 4
-            s1[zz, yy] = (dwb[i, c].astype(F32) + crecv[i].astype(F32)).astype(BF)
+            s1[zz, yy] = dwb[i, c] + crecv[i]
             return carry
 
-        lax.fori_loop(0, 16, body, 0)
+        lax.fori_loop(0, 16, body, 0, unroll=2)
         f, u = ("f", m), ("u", m)
         send(s1.at[lo, yid[2], ra], fold.at[0, lo], ydev[1], f, f)
         send(s1.at[hi, yid[2], ra], fold.at[0, hi], ydev[3], f, f)
@@ -295,7 +295,7 @@
         for i in range(4):
             r = 1 if i < LO else 3
             for part, at in enumerate(((i, yid[r], ra), (zid[r], i, rb))):
-                s1[at] = (s1[at].astype(F32) + fold[part, i].astype(F32)).astype(BF)
+                s1[at] = s1[at] + fold[part, i]
         send(s1.at[lo, yid[1], ra], recv2.at[0, lo], ydev[1], u, u)
         send(s1.at[hi, yid[3], ra], recv2.at[1, hi], ydev[3], u, u)
         send(s1.at[zid[1], lo, rb], recv2.at[2, lo], zdev[1], u, u)
@@ -348,8 +348,8 @@
 
     def dx_folded(t):
         arrived(("df", t), dx_fold.at[t])
-        dx_send[t, 4] = (dx_part[t, 0].astype(F32) + dx_fold[t, 0].astype(F32)).astype(BF)
-        dx_send[t, 5] = (dx_part[t, 1].astype(F32) + dx_fold[t, 1].astype(F32)).astype(BF)
+        dx_send[t, 4] = dx_part[t, 0] + dx_fold[t, 0]
+        dx_send[t, 5] = dx_part[t, 1] + dx_fold[t, 1]
         send(dx_send.at[t, 4], dx_recv.at[t, 0, half_a], right, "d", ("d", t))
         send(dx_send.at[t, 5], dx_recv.at[t, 1, half_b], left, "d", ("d", t))
 
@@ -399,34 +399,34 @@
     rs_start(1)
     weight_grad(2)
     dx_direct(1)
-    rs_start(2)
     bias_line()
     send(gl, gl_c, partner, "gc", "gc")
+    rs_start(2)
     rs_second(0)
-    rs_fold(1)
     arrived("gc", gl_c)
     gl_s[0] = gl[...] + gl_c[...]
     for r in (1, 2, 3):
         send(gl_s.at[0], gl_r.at[r - 1], ydev[r], "gr", "gy")
+    rs_fold(1)
     dx_folded(1)
     dx_mine()
     rs_fold(2)
     dx_finish(0)
-    rs_second(1)
-    rs_second(2)
     arrived("gy", gl_r.at[pl.ds(0, 3)])
     gl_s[1] = gl_s[0] + gl_r[0] + gl_r[1] + gl_r[2]
     for r in (1, 2, 3):
         send(gl_s.at[1], gl_r.at[2 + r], zdev[r], "gr", "gz")
+    rs_second(1)
+    rs_second(2)
     rs_finish(0)
-    dx_finish(1)
-    rs_finish(1)
     arrived("gz", gl_r.at[pl.ds(3, 3)])
     total = gl_s[1] + gl_r[3] + gl_r[4] + gl_r[5]
     far = jnp.sum(jnp.where(lane < 128, total, 0.0), axis=1, keepdims=True)
     total = jnp.where(lane == 0, far, total)
     total = pltpu.roll(total, 512 - 193, 1)
     gb_ref[...] = total[0:6, 0:320]
+    rs_finish(1)
+    dx_finish(1)
     rs_finish(2)
     sent("x", xbuf.at[:, pl.ds(0, 2304)])
     sent("h", kext.at[:, pl.ds(0, 512)])

time: 73 us -> 72.6 us (level)
  no operation moved by 1% of the time
where the time goes in v4:
time: 72.6 us; the launch traced here: 72.4 us
  Pallas kernels  71.6 us (99%)
  between operations  0.82 us (1%)
    pallas_call x1, Pallas kernels, local(): pl.pallas_call(kernel, out_shape=(V((512, 768), BF), V((96, 1152), F32),...  70.5 us

profile of v4, /device:TPU:0, one launch (start us, length us, event | category | flops | bytes accessed | tf_op | source)
XLA Modules:
  0.0 72.4 jit_solution(6966118764183764156)
XLA Ops:
  0.6 70.5 %shard_map.101 = (bf16[512,768]{1,0:T(8,128)(2,1)S(1)}, f32[96,1152]{1,0:T(8,128)S(1)}, f32[6,320]{1,0:T(8,128)S(1)}) custom-call(bf16[512,768]{1,0:T(8,128)(2,1)} %x_hbm.1, bf16[3072,384]{1,0:T(8,128)(2,1)} %wq_hbm.1, bf16[3072,384]{1,0:T(8,128)(2,1)} %wk_hbm.1, bf16[3072,384]{1,0:T(8,128)(2,1)} %wv_hbm.1, f32[6,320]{1,0:T(8,128)} %bitcast.2, ...), custom_call_target="tpu_custom_call" | custom-call | tf_op jit(solution)/shard_map/pallas_call | solution.py:463
  71.2 1.1 %shard_map.102 = (bf16[512,768]{1,0:T(8,128)(2,1)}, f32[96,384]{1,0:T(8,128)}, f32[96,384]{1,0:T(8,128)}, f32[96,384]{1,0:T(8,128)}, f32[6,320]{1,0:T(8,128)}) custom-call(bf16[512,768]{1,0:T(8,128)(2,1)S(1)} %get-tuple-element.13.gx, f32[96,1152]{1,0:T(8,128)S(1)} %get-tuple-element.14.gw, f32[6,320]{1,0:T(8,128)S(1)} %get-tuple-element.15.gb), custom_call_target="tpu_custom_call" | custom-call | tf_op jit(solution)/shard_map/pallas_call | solution.py:513
